TPU v7x, 32 devices: a whole 2x2x4 slice. The times are simulated.
32 devices in a mesh: pp: 4 (over y, x), tp: 8 (over z, core).
Axes of the slice: x: 2, y: 2, z: 4, core: 2. Of those that a mesh axis runs over, the one named last changes fastest.
Arguments:
- entry_stream_rows: bfloat16 [256, 2048], P('pp', 'tp'), may hold values from -21 to 21
- layer_rescale_factor: float32 [4, 2048], P('pp'), may hold values from 0.1 to 1.9
- probe_projection: bfloat16 [4, 2048, 2048], P('pp', 'tp'), may hold values from -0.125 to 0.125
- retention_projection: bfloat16 [4, 2048, 2048], P('pp', 'tp'), may hold values from -0.125 to 0.125
- candidate_projection: bfloat16 [4, 2048, 2048], P('pp', 'tp'), may hold values from -0.125 to 0.125
- emission_filter_matrix: bfloat16 [4, 2048, 2048], P('pp', 'tp'), may hold values from -0.125 to 0.125
- retention_minimum: float32 [4, 2048], P('pp', 'tp'), may hold values from 0.88 to 0.9921875
- decay_spike: float32 [4, 128, 32], P('pp', None, 'tp'), may hold values from -2.1 to 0
- per_group_scale: float32 [4, 64], P('pp'), may hold values from 0.1 to 1.9
Outputs:
- outputs: bfloat16 [256, 2048], P('pp', 'tp')
All inputs are finite; a program needn't handle non-finite values.
Results may differ from a plain program's by a relative error of at most 0.03.
Values may be sent and summed in bfloat16 or wider, within the bound.
A program may use at most 64 MiB of HBM per device.

v0:
```python
import jax
import jax.numpy as jnp
from jax import lax
from jax.sharding import PartitionSpec as P

HEAD = 64
SEG = 64
EPSILON = 1e-06
HIGHEST = lax.Precision.HIGHEST


def shifted(array, axis, by):
    devices = lax.axis_size(axis)
    pairs = [(i, i + by) for i in range(devices) if 0 <= i + by < devices]
    return lax.ppermute(array, axis, pairs)


def spread(value, axis, source):
    kept = jnp.where(lax.axis_index(axis) == source, value, 0).astype(value.dtype)
    return lax.psum(kept, axis)


def segment_scan(queries, key_in, log_forget, values, memory):
    head_count = queries.shape[0]
    length = queries.shape[1]
    blocks_count = length // SEG

    def split_blocks(tensor):
        return tensor.reshape(head_count, blocks_count, SEG, tensor.shape[-1]).transpose(1, 0, 2, 3)

    lower_mask = jnp.tril(jnp.ones((SEG, SEG), dtype=bool))[None]

    def one_block(memory_in, pieces):
        block_query, block_key, block_forget, block_value = pieces
        running = jnp.cumsum(block_forget, axis=1)
        query_scaled = block_query * jnp.exp(running)
        key_scaled = block_key * jnp.exp(-running)
        scores = jnp.einsum("hid,hjd->hij", query_scaled, key_scaled, precision=HIGHEST)
        scores = jnp.where(lower_mask, scores, 0.0)
        mixed_out = jnp.einsum("hij,hjv->hiv", scores, block_value, precision=HIGHEST)
        mixed_out = mixed_out + jnp.einsum(
            "hid,hdv->hiv", query_scaled, memory_in, precision=HIGHEST
        )
        ending = running[:, -1:, :]
        carried_in = jnp.einsum(
            "hjd,hjv->hdv", block_key * jnp.exp(ending - running), block_value, precision=HIGHEST
        )
        memory_out = jnp.exp(ending[:, 0, :])[:, :, None] * memory_in + carried_in
        return (memory_out, mixed_out)

    memory, mixed_out = lax.scan(
        one_block,
        memory,
        (
            split_blocks(queries),
            split_blocks(key_in),
            split_blocks(log_forget),
            split_blocks(values),
        ),
    )
    return (mixed_out.transpose(1, 0, 2, 3).reshape(head_count, length, values.shape[-1]), memory)


def head_norm(mixed_out, channel_gain):
    return (
        mixed_out
        * lax.rsqrt(jnp.mean(mixed_out * mixed_out, axis=-1, keepdims=True) + EPSILON)
        * channel_gain
    )


def shards(
    entry_stream_rows,
    layer_rescale_factor,
    probe_projection,
    retention_projection,
    candidate_projection,
    emission_filter_matrix,
    retention_minimum,
    decay_spike,
    per_group_scale,
):
    sections = lax.axis_size("pp")
    layer_ordinal = lax.axis_index("pp")
    own_rows = entry_stream_rows.shape[0]
    seq_len = 2 * own_rows
    columns = entry_stream_rows.shape[1]
    head_here = columns // HEAD
    model_width = layer_rescale_factor.shape[1]
    micro_count = sections // 2
    per_sequence = seq_len // seq_len
    unit_count = micro_count * per_sequence
    total_steps = unit_count + sections - 1
    entering = lax.all_gather(entry_stream_rows, "pp", axis=0, tiled=True)
    weights = jnp.concatenate(
        [
            probe_projection[0],
            retention_projection[0],
            candidate_projection[0],
            emission_filter_matrix[0],
        ],
        axis=0,
    )
    input_gain = layer_rescale_factor[0]
    lower_edge = retention_minimum[0].reshape(head_here, 1, HEAD)
    spike_collection = decay_spike[0].T
    out_gain = per_group_scale[0]

    def add_piece(piece_in):
        wide_piece = piece_in.astype(jnp.float32)
        scaled = (wide_piece * input_gain[None, :]).astype(jnp.bfloat16)
        product = lax.dot_general(
            scaled, weights, (((1,), (1,)), ((), ())), preferred_element_type=jnp.float32
        )
        return (product, jnp.sum(wide_piece * wide_piece, axis=1))

    def one_step(step_index, carried):
        incoming, memory, finished = carried
        unit_index = step_index - layer_ordinal
        first_slot = jnp.clip(step_index, 0, unit_count - 1)
        fresh_rows = lax.dynamic_slice_in_dim(entering, first_slot * seq_len, seq_len, 0)
        current = jnp.where(layer_ordinal == 0, fresh_rows, incoming)
        projected, squares = add_piece(lax.all_gather(current, "tp", axis=1, tiled=True))
        inverse = lax.rsqrt(squares / model_width + EPSILON)[:, None]
        projected = projected * inverse

        def per_head(role_index):
            picked = projected[:, role_index * columns : (role_index + 1) * columns]
            return picked.reshape(seq_len, head_here, HEAD).transpose(1, 0, 2)

        query_pre = per_head(0)
        forget_pre = per_head(1)
        input_pre = per_head(2)
        gate_pre = per_head(3)
        offset = unit_index % per_sequence * seq_len
        current_surge = spike_collection[:, :, None]
        log_forget = (
            jnp.logaddexp(
                jnp.log(lower_edge), jnp.log1p(-lower_edge) + jax.nn.log_sigmoid(forget_pre)
            )
            + current_surge
        )
        key_in = (1.0 - lower_edge) * jax.nn.sigmoid(-forget_pre)
        queries = jax.nn.silu(query_pre)
        memory = jnp.where(offset == 0, jnp.zeros_like(memory), memory)
        mixed_out, memory = segment_scan(queries, key_in, log_forget, input_pre, memory)
        branch = head_norm(mixed_out, out_gain) * jax.nn.silu(gate_pre)
        branch = branch.transpose(1, 0, 2).reshape(seq_len, columns)
        result = (current.astype(jnp.float32) + branch).astype(jnp.bfloat16)
        passed = shifted(result, "pp", 1)
        out_slot = jnp.clip(unit_index, 0, unit_count - 1)
        write_here = (layer_ordinal == sections - 1) & (unit_index >= 0) & (unit_index < unit_count)
        updated = lax.dynamic_update_slice_in_dim(finished, result, out_slot * seq_len, 0)
        finished = jnp.where(write_here, updated, finished)
        return (passed, memory, finished)

    start_state = (
        jnp.zeros((seq_len, columns), jnp.bfloat16),
        jnp.zeros((head_here, HEAD, HEAD), jnp.float32),
        jnp.zeros((unit_count * seq_len, columns), jnp.bfloat16),
    )
    carried_out = lax.fori_loop(0, total_steps, one_step, start_state)
    everything = spread(carried_out[2], "pp", sections - 1)
    return lax.dynamic_slice_in_dim(everything, layer_ordinal * own_rows, own_rows, 0)


def solution(mesh):
    in_specs = (
        P("pp", "tp"),
        P("pp", None),
        P("pp", "tp", None),
        P("pp", "tp", None),
        P("pp", "tp", None),
        P("pp", "tp", None),
        P("pp", "tp"),
        P("pp", None, "tp"),
        P("pp", None),
    )
    out_specs = P("pp", "tp")
    return jax.shard_map(shards, mesh=mesh, in_specs=in_specs, out_specs=out_specs, check_vma=False)
```

profile of v0, /device:TPU:0, one launch (start us, length us, event | category | flops | bytes accessed | tf_op | source)
XLA Modules:
  0.0 245.3 jit_solution(12410205212231642517)
XLA Ops:
  8.6 10.1 %all_gather.14 = bf16[256,256]{1,0:T(8,128)(2,1)S(1)} all-gather(bf16[64,256]{1,0:T(8,128)(2,1)} %param.13), channel_id=1, replica_groups=mesh['pp'=4,'tp'=8] {'pp'}, dimensions={0}, use_global_device_ids=true | all-gather | bytes 163840 | tf_op jit(solution)/shard_map/all_gather | solution.py:94
  18.8 3.7 %pad_maximum_fusion = bf16[1024,2048]{1,0:T(8,128)(2,1)} fusion(bf16[256,2048]{1,0:T(8,128)(2,1)} %bitcast.150, bf16[256,2048]{1,0:T(8,128)(2,1)} %bitcast.151, bf16[256,2048]{1,0:T(8,128)(2,1)} %bitcast.152, bf16[256,2048]{1,0:T(8,128)(2,1)} %bitcast.153), kind=kLoop, calls=%fused_computation.50 | loop fusion | flops 16777216 | bytes 8388608 | tf_op jit(solution)/shard_map/concatenate | solution.py:95
  22.5 167.6 %while.59 = (s32[]{:T(128)}, bf16[128,256]{0,1:T(8,128)(2,1)S(1)}, bf16[256,256]{1,0:T(8,128)(2,1)S(1)}, pred[]{:T(512)}, bf16[256,256]{1,0:T(8,128)(2,1)S(1)}, ...) while((s32[]{:T(128)}, bf16[128,256]{0,1:T(8,128)(2,1)S(1)}, ...), condition=%wide.region_6.7_spmd, body=%wide.region_0.6_spmd.sunk | while | flops 591418240 | bytes 15908739 | solution.py:162
  22.8 15.2 %all_gather.16 = bf16[128,2048]{0,1:T(8,128)(2,1)S(1)} all-gather(bf16[128,256]{0,1:T(8,128)(2,1)S(1)} %broadcast_select_fusion.5), channel_id=1, replica_groups=mesh['pp'=4,'tp'=8] {'tp'}, dimensions={1}, use_global_device_ids=true | all-gather | bytes 589824 | tf_op jit(solution)/shard_map/while/body/eval_jaxpr/all_gather | solution.py:123
  38.2 4.2 %convolution_multiply_fusion.2 = f32[128,1024]{1,0:T(8,128)S(1)} fusion(bf16[1024,2048]{1,0:T(8,128)(2,1)} %get-tuple-element.759, bf16[128,2048]{0,1:T(8,128)(2,1)S(1)} %all_gather.16, f32[2048]{0:T(1024)S(1)} %bitcast.154, f32[128]{0:T(128)S(1)} %add_rsqrt_fusion.4), kind=kOutput, calls=%fused_computation.26.clone.1 | convolution fusion | flops 537788416 | bytes 5251584 | tf_op jit(solution)/shard_map/while/body/eval_jaxpr/dot_general | solution.py:112
  44.0 5.0 %while.60 = (s32[]{:T(128)}, f32[4,64,64]{2,1,0:T(8,128)S(1)}, f32[2,4,64,64]{3,2,1,0:T(8,128)S(1)}, f32[2,4,64,64]{2,0,3,1:T(2,128)S(1)}, f32[2,4,64,64]{2,0,3,...) while((s32[]{:T(128)}, f32[4,64,64]{2,1,0:T(8,128)S(1)}, ...), condition=%wide.region_4.4_spmd.clone, body=%wide.region_2.3_spmd.clone.sunk | while | flops 51564544 | bytes 2504832 | solution.py:51
  50.0 3.2 %collective-permute-start = (bf16[128,256]{0,1:T(8,128)(2,1)S(1)}, bf16[128,256]{0,1:T(8,128)(2,1)S(1)}, u32[]{:S(2)}, u32[]{:S(2)}) collective-permute-start(bf16[128,256]{0,1:T(8,128)(2,1)S(1)} %get-tuple-element.665), channel_id=1, source_target_pairs={{0,8},{8,16},{16,24},{1,9},{9,17},{17,25},{2,10},{10,18},{18,26},{... | collective-permute-start | bytes 196616 | tf_op jit(solution)/shard_map/while/body/eval_jaxpr/ppermute | solution.py:15
  55.2 14.7 %all_gather.16 = bf16[128,2048]{0,1:T(8,128)(2,1)S(1)} all-gather(bf16[128,256]{0,1:T(8,128)(2,1)S(1)} %broadcast_select_fusion.5), channel_id=1, replica_groups=mesh['pp'=4,'tp'=8] {'tp'}, dimensions={1}, use_global_device_ids=true | all-gather | bytes 589824 | tf_op jit(solution)/shard_map/while/body/eval_jaxpr/all_gather | solution.py:123
  70.2 4.2 %convolution_multiply_fusion.2 = f32[128,1024]{1,0:T(8,128)S(1)} fusion(bf16[1024,2048]{1,0:T(8,128)(2,1)} %get-tuple-element.759, bf16[128,2048]{0,1:T(8,128)(2,1)S(1)} %all_gather.16, f32[2048]{0:T(1024)S(1)} %bitcast.154, f32[128]{0:T(128)S(1)} %add_rsqrt_fusion.4), kind=kOutput, calls=%fused_computation.26.clone.1 | convolution fusion | flops 537788416 | bytes 5251584 | tf_op jit(solution)/shard_map/while/body/eval_jaxpr/dot_general | solution.py:112
  76.0 5.0 %while.60 = (s32[]{:T(128)}, f32[4,64,64]{2,1,0:T(8,128)S(1)}, f32[2,4,64,64]{3,2,1,0:T(8,128)S(1)}, f32[2,4,64,64]{2,0,3,1:T(2,128)S(1)}, f32[2,4,64,64]{2,0,3,...) while((s32[]{:T(128)}, f32[4,64,64]{2,1,0:T(8,128)S(1)}, ...), condition=%wide.region_4.4_spmd.clone, body=%wide.region_2.3_spmd.clone.sunk | while | flops 51564544 | bytes 2504832 | solution.py:51
  82.0 4.3 %collective-permute-start = (bf16[128,256]{0,1:T(8,128)(2,1)S(1)}, bf16[128,256]{0,1:T(8,128)(2,1)S(1)}, u32[]{:S(2)}, u32[]{:S(2)}) collective-permute-start(bf16[128,256]{0,1:T(8,128)(2,1)S(1)} %get-tuple-element.665), channel_id=1, source_target_pairs={{0,8},{8,16},{16,24},{1,9},{9,17},{17,25},{2,10},{10,18},{18,26},{... | collective-permute-start | bytes 196616 | tf_op jit(solution)/shard_map/while/body/eval_jaxpr/ppermute | solution.py:15
  88.3 15.0 %all_gather.16 = bf16[128,2048]{0,1:T(8,128)(2,1)S(1)} all-gather(bf16[128,256]{0,1:T(8,128)(2,1)S(1)} %broadcast_select_fusion.5), channel_id=1, replica_groups=mesh['pp'=4,'tp'=8] {'tp'}, dimensions={1}, use_global_device_ids=true | all-gather | bytes 589824 | tf_op jit(solution)/shard_map/while/body/eval_jaxpr/all_gather | solution.py:123
  103.6 4.2 %convolution_multiply_fusion.2 = f32[128,1024]{1,0:T(8,128)S(1)} fusion(bf16[1024,2048]{1,0:T(8,128)(2,1)} %get-tuple-element.759, bf16[128,2048]{0,1:T(8,128)(2,1)S(1)} %all_gather.16, f32[2048]{0:T(1024)S(1)} %bitcast.154, f32[128]{0:T(128)S(1)} %add_rsqrt_fusion.4), kind=kOutput, calls=%fused_computation.26.clone.1 | convolution fusion | flops 537788416 | bytes 5251584 | tf_op jit(solution)/shard_map/while/body/eval_jaxpr/dot_general | solution.py:112
  109.4 5.0 %while.60 = (s32[]{:T(128)}, f32[4,64,64]{2,1,0:T(8,128)S(1)}, f32[2,4,64,64]{3,2,1,0:T(8,128)S(1)}, f32[2,4,64,64]{2,0,3,1:T(2,128)S(1)}, f32[2,4,64,64]{2,0,3,...) while((s32[]{:T(128)}, f32[4,64,64]{2,1,0:T(8,128)S(1)}, ...), condition=%wide.region_4.4_spmd.clone, body=%wide.region_2.3_spmd.clone.sunk | while | flops 51564544 | bytes 2504832 | solution.py:51
  115.4 4.3 %collective-permute-start = (bf16[128,256]{0,1:T(8,128)(2,1)S(1)}, bf16[128,256]{0,1:T(8,128)(2,1)S(1)}, u32[]{:S(2)}, u32[]{:S(2)}) collective-permute-start(bf16[128,256]{0,1:T(8,128)(2,1)S(1)} %get-tuple-element.665), channel_id=1, source_target_pairs={{0,8},{8,16},{16,24},{1,9},{9,17},{17,25},{2,10},{10,18},{18,26},{... | collective-permute-start | bytes 196616 | tf_op jit(solution)/shard_map/while/body/eval_jaxpr/ppermute | solution.py:15
  121.8 14.9 %all_gather.16 = bf16[128,2048]{0,1:T(8,128)(2,1)S(1)} all-gather(bf16[128,256]{0,1:T(8,128)(2,1)S(1)} %broadcast_select_fusion.5), channel_id=1, replica_groups=mesh['pp'=4,'tp'=8] {'tp'}, dimensions={1}, use_global_device_ids=true | all-gather | bytes 589824 | tf_op jit(solution)/shard_map/while/body/eval_jaxpr/all_gather | solution.py:123
  137.0 4.2 %convolution_multiply_fusion.2 = f32[128,1024]{1,0:T(8,128)S(1)} fusion(bf16[1024,2048]{1,0:T(8,128)(2,1)} %get-tuple-element.759, bf16[128,2048]{0,1:T(8,128)(2,1)S(1)} %all_gather.16, f32[2048]{0:T(1024)S(1)} %bitcast.154, f32[128]{0:T(128)S(1)} %add_rsqrt_fusion.4), kind=kOutput, calls=%fused_computation.26.clone.1 | convolution fusion | flops 537788416 | bytes 5251584 | tf_op jit(solution)/shard_map/while/body/eval_jaxpr/dot_general | solution.py:112
  142.7 5.0 %while.60 = (s32[]{:T(128)}, f32[4,64,64]{2,1,0:T(8,128)S(1)}, f32[2,4,64,64]{3,2,1,0:T(8,128)S(1)}, f32[2,4,64,64]{2,0,3,1:T(2,128)S(1)}, f32[2,4,64,64]{2,0,3,...) while((s32[]{:T(128)}, f32[4,64,64]{2,1,0:T(8,128)S(1)}, ...), condition=%wide.region_4.4_spmd.clone, body=%wide.region_2.3_spmd.clone.sunk | while | flops 51564544 | bytes 2504832 | solution.py:51
  148.7 5.2 %collective-permute-start = (bf16[128,256]{0,1:T(8,128)(2,1)S(1)}, bf16[128,256]{0,1:T(8,128)(2,1)S(1)}, u32[]{:S(2)}, u32[]{:S(2)}) collective-permute-start(bf16[128,256]{0,1:T(8,128)(2,1)S(1)} %get-tuple-element.665), channel_id=1, source_target_pairs={{0,8},{8,16},{16,24},{1,9},{9,17},{17,25},{2,10},{10,18},{18,26},{... | collective-permute-start | bytes 196616 | tf_op jit(solution)/shard_map/while/body/eval_jaxpr/ppermute | solution.py:15
  155.9 15.0 %all_gather.16 = bf16[128,2048]{0,1:T(8,128)(2,1)S(1)} all-gather(bf16[128,256]{0,1:T(8,128)(2,1)S(1)} %broadcast_select_fusion.5), channel_id=1, replica_groups=mesh['pp'=4,'tp'=8] {'tp'}, dimensions={1}, use_global_device_ids=true | all-gather | bytes 589824 | tf_op jit(solution)/shard_map/while/body/eval_jaxpr/all_gather | solution.py:123
  171.2 4.2 %convolution_multiply_fusion.2 = f32[128,1024]{1,0:T(8,128)S(1)} fusion(bf16[1024,2048]{1,0:T(8,128)(2,1)} %get-tuple-element.759, bf16[128,2048]{0,1:T(8,128)(2,1)S(1)} %all_gather.16, f32[2048]{0:T(1024)S(1)} %bitcast.154, f32[128]{0:T(128)S(1)} %add_rsqrt_fusion.4), kind=kOutput, calls=%fused_computation.26.clone.1 | convolution fusion | flops 537788416 | bytes 5251584 | tf_op jit(solution)/shard_map/while/body/eval_jaxpr/dot_general | solution.py:112
  177.0 5.0 %while.60 = (s32[]{:T(128)}, f32[4,64,64]{2,1,0:T(8,128)S(1)}, f32[2,4,64,64]{3,2,1,0:T(8,128)S(1)}, f32[2,4,64,64]{2,0,3,1:T(2,128)S(1)}, f32[2,4,64,64]{2,0,3,...) while((s32[]{:T(128)}, f32[4,64,64]{2,1,0:T(8,128)S(1)}, ...), condition=%wide.region_4.4_spmd.clone, body=%wide.region_2.3_spmd.clone.sunk | while | flops 51564544 | bytes 2504832 | solution.py:51
  183.0 5.2 %collective-permute-start = (bf16[128,256]{0,1:T(8,128)(2,1)S(1)}, bf16[128,256]{0,1:T(8,128)(2,1)S(1)}, u32[]{:S(2)}, u32[]{:S(2)}) collective-permute-start(bf16[128,256]{0,1:T(8,128)(2,1)S(1)} %get-tuple-element.665), channel_id=1, source_target_pairs={{0,8},{8,16},{16,24},{1,9},{9,17},{17,25},{2,10},{10,18},{18,26},{... | collective-permute-start | bytes 196616 | tf_op jit(solution)/shard_map/while/body/eval_jaxpr/ppermute | solution.py:15
  190.8 46.3 %all-reduce.2.cloned.1.call-done = bf16[256,256]{1,0:T(8,128)(2,1)} async-done(((bf16[256,256]{1,0:T(8,128)(2,1)}), bf16[256,256]{1,0:T(8,128)(2,1)}) %all-reduce.2.cloned.1.call-update) | async-done | bytes 131088 | tf_op jit(solution)/shard_map/psum | solution.py:20
  (316 shorter events, 51.6 us)
Async XLA Ops:
  6.5 230.5 %all-reduce.2.cloned.1.call-start = ((), (), s32[]{:S(2)}) async-start(), calls=%async_computation | async-start | bytes 262144 | tf_op jit(solution)/shard_map/psum | solution.py:20
  18.7 3.8 %copy-start = (f32[1,2048]{1,0:T(1,128)S(1)}, f32[1,2048]{1,0:T(1,128)}, u32[]{:S(2)}) copy-start(f32[1,2048]{1,0:T(1,128)} %param.14) | copy-start | bytes 24580
  18.7 3.8 %copy-start.1 = (f32[1,128,4]{1,2,0:T(4,128)S(1)}, f32[1,128,4]{1,2,0:T(4,128)}, u32[]{:S(2)}) copy-start(f32[1,128,4]{1,2,0:T(4,128)} %param.20) | copy-start | bytes 6148
  18.8 3.8 %copy-start.2 = (f32[1,64]{1,0:T(1,128)S(1)}, f32[1,64]{1,0:T(1,128)}, u32[]{:S(2)}) copy-start(f32[1,64]{1,0:T(1,128)} %param.21) | copy-start | bytes 772
  50.0 5.1 %collective-permute-start = (bf16[128,256]{0,1:T(8,128)(2,1)S(1)}, bf16[128,256]{0,1:T(8,128)(2,1)S(1)}, u32[]{:S(2)}, u32[]{:S(2)}) collective-permute-start(bf16[128,256]{0,1:T(8,128)(2,1)S(1)} %get-tuple-element.665), channel_id=1, source_target_pairs={{0,8},{8,16},{16,24},{1,9},{9,17},{17,25},{2,10},{10,18},{18,26},{... | collective-permute-start | bytes 196616 | tf_op jit(solution)/shard_map/while/body/eval_jaxpr/ppermute | solution.py:15
  82.0 6.2 %collective-permute-start = (bf16[128,256]{0,1:T(8,128)(2,1)S(1)}, bf16[128,256]{0,1:T(8,128)(2,1)S(1)}, u32[]{:S(2)}, u32[]{:S(2)}) collective-permute-start(bf16[128,256]{0,1:T(8,128)(2,1)S(1)} %get-tuple-element.665), channel_id=1, source_target_pairs={{0,8},{8,16},{16,24},{1,9},{9,17},{17,25},{2,10},{10,18},{18,26},{... | collective-permute-start | bytes 196616 | tf_op jit(solution)/shard_map/while/body/eval_jaxpr/ppermute | solution.py:15
  115.4 6.2 %collective-permute-start = (bf16[128,256]{0,1:T(8,128)(2,1)S(1)}, bf16[128,256]{0,1:T(8,128)(2,1)S(1)}, u32[]{:S(2)}, u32[]{:S(2)}) collective-permute-start(bf16[128,256]{0,1:T(8,128)(2,1)S(1)} %get-tuple-element.665), channel_id=1, source_target_pairs={{0,8},{8,16},{16,24},{1,9},{9,17},{17,25},{2,10},{10,18},{18,26},{... | collective-permute-start | bytes 196616 | tf_op jit(solution)/shard_map/while/body/eval_jaxpr/ppermute | solution.py:15
  148.7 7.1 %collective-permute-start = (bf16[128,256]{0,1:T(8,128)(2,1)S(1)}, bf16[128,256]{0,1:T(8,128)(2,1)S(1)}, u32[]{:S(2)}, u32[]{:S(2)}) collective-permute-start(bf16[128,256]{0,1:T(8,128)(2,1)S(1)} %get-tuple-element.665), channel_id=1, source_target_pairs={{0,8},{8,16},{16,24},{1,9},{9,17},{17,25},{2,10},{10,18},{18,26},{... | collective-permute-start | bytes 196616 | tf_op jit(solution)/shard_map/while/body/eval_jaxpr/ppermute | solution.py:15
  183.0 7.1 %collective-permute-start = (bf16[128,256]{0,1:T(8,128)(2,1)S(1)}, bf16[128,256]{0,1:T(8,128)(2,1)S(1)}, u32[]{:S(2)}, u32[]{:S(2)}) collective-permute-start(bf16[128,256]{0,1:T(8,128)(2,1)S(1)} %get-tuple-element.665), channel_id=1, source_target_pairs={{0,8},{8,16},{16,24},{1,9},{9,17},{17,25},{2,10},{10,18},{18,26},{... | collective-permute-start | bytes 196616 | tf_op jit(solution)/shard_map/while/body/eval_jaxpr/ppermute | solution.py:15
Sparse Core Ops, SparseCore 0:
  190.9 46.0 all-reduce.1
where the time goes:
time: 246 us; the launch traced here: 245 us
  blocking collectives  84.9 us (35%)
  waiting for transfers between devices  55 us (22%)
  matrix products  34.7 us (14%)
  starting transfers between devices  22.3 us (9%)
  local copies, waits for them, and re-layouts  20.5 us (8%)
  between operations  13.4 us (5%)
  other arithmetic  12.1 us (5%)
    all_gather x5, blocking collectives, one_step(): lax.all_gather(current, 'tp', axis=1, tiled=True)  74.8 us
    psum x1, waiting for transfers between devices, spread(): return lax.psum(kept, axis)  46.3 us
    ppermute x5, starting transfers between devices, shifted(): return lax.ppermute(array, axis, pairs)  22.3 us
    dot_general x5, matrix products, add_piece(): lax.dot_general(scaled, weights, (((1,), (1,)), ((), ())), preferred_elem...  20.8 us
    all_gather x1, blocking collectives, shards(): entering = lax.all_gather(entry_stream_rows, 'pp', axis=0, tiled=True)  10.1 us
    ppermute x5, waiting for transfers between devices, shifted(): return lax.ppermute(array, axis, pairs)  8.75 us
    dynamic_slice x50, local copies, waits for them, and re-layouts, segment_scan(): lax.scan(one_block, memory, (split_blocks(queries), split_blocks(key_in),...  8.32 us
  transfers between devices with their start and end apart: 6, of which 6 were waited for; matrix products, arithmetic and copies ran while one was open for 0% of the time, Pallas kernels for 0%

commit v1 on v0

--- a/solution.py
+++ b/solution.py
@@ -17,7 +17,7 @@
 
 def spread(value, axis, source):
     kept = jnp.where(lax.axis_index(axis) == source, value, 0).astype(value.dtype)
-    return lax.psum(kept, axis)
+    return jnp.sum(lax.all_gather(kept, axis), axis=0)
 
 
 def segment_scan(queries, key_in, log_forget, values, memory):

time: 246 us -> 201 us (0.82)
  waiting for transfers between devices: 55 us -> 9.41 us
  blocking collectives: 84.9 us -> 101 us
  between operations: 13.4 us -> 0.09 us
    psum x1 -> x0, waiting for transfers between devices: 46.3 us -> none  [spread(): return lax.psum(kept, axis)]
    all_gather x0 -> x1, blocking collectives: none -> 16.3 us  [spread(): return jnp.sum(lax.all_gather(kept, axis), axis=0)]
  transfers between devices with their start and end apart: 6 -> 5, of which waited for: 6 -> 5; matrix products, arithmetic and copies ran while one was open for 0% -> 0% of each run, Pallas kernels for 0% -> 0%
where the time goes in v1:
time: 201 us
  blocking collectives  101 us (50%)
  matrix products  34.7 us (17%)
  starting transfers between devices  22.4 us (11%)
  local copies, waits for them, and re-layouts  19 us (9%)
  other arithmetic  12.2 us (6%)
  waiting for transfers between devices  9.41 us (5%)
  loops' own time  2.08 us (1%)
    all_gather x5, blocking collectives, one_step(): lax.all_gather(current, 'tp', axis=1, tiled=True)  74.8 us
    ppermute x5, starting transfers between devices, shifted(): return lax.ppermute(array, axis, pairs)  22.4 us
    dot_general x5, matrix products, add_piece(): lax.dot_general(scaled, weights, (((1,), (1,)), ((), ())), preferred_elem...  20.8 us
    all_gather x1, blocking collectives, spread(): return jnp.sum(lax.all_gather(kept, axis), axis=0)  16.3 us
    all_gather x1, blocking collectives, shards(): entering = lax.all_gather(entry_stream_rows, 'pp', axis=0, tiled=True)  9.93 us
    ppermute x5, waiting for transfers between devices, shifted(): return lax.ppermute(array, axis, pairs)  9.41 us
    dynamic_slice x50, local copies, waits for them, and re-layouts, segment_scan(): lax.scan(one_block, memory, (split_blocks(queries), split_blocks(key_in),...  8.32 us
    dot_general x10, matrix products, one_block(): jnp.einsum('hjd,hjv->hdv', block_key * jnp.exp(ending - running), block_v...  4.14 us
  transfers between devices with their start and end apart: 5, of which 5 were waited for; matrix products, arithmetic and copies ran while one was open for 0% of the time, Pallas kernels for 0%

profile of v1, /device:TPU:0, one launch (start us, length us, event | category | flops | bytes accessed | tf_op | source)
XLA Modules:
  0.0 201.0 jit_solution(2899185413569783871)
XLA Ops:
  2.0 3.7 %pad_maximum_fusion = bf16[1024,2048]{1,0:T(8,128)(2,1)} fusion(bf16[256,2048]{1,0:T(8,128)(2,1)} %bitcast.151, bf16[256,2048]{1,0:T(8,128)(2,1)} %bitcast.152, bf16[256,2048]{1,0:T(8,128)(2,1)} %bitcast.153, bf16[256,2048]{1,0:T(8,128)(2,1)} %bitcast.154), kind=kLoop, calls=%fused_computation.48 | loop fusion | flops 16777216 | bytes 8388608 | tf_op jit(solution)/shard_map/concatenate | solution.py:95
  5.7 9.9 %all_gather.20 = bf16[256,256]{1,0:T(8,128)(2,1)S(1)} all-gather(bf16[64,256]{1,0:T(8,128)(2,1)S(1)} %copy-done.2), channel_id=1, replica_groups=mesh['pp'=4,'tp'=8] {'pp'}, dimensions={0}, use_global_device_ids=true | all-gather | bytes 163840 | tf_op jit(solution)/shard_map/all_gather | solution.py:94
  15.7 167.1 %while.59 = (s32[]{:T(128)}, bf16[128,256]{0,1:T(8,128)(2,1)S(1)}, bf16[256,256]{0,1:T(8,128)(2,1)S(1)}, pred[]{:T(512)}, bf16[256,256]{1,0:T(8,128)(2,1)S(1)}, ...) while((s32[]{:T(128)}, bf16[128,256]{0,1:T(8,128)(2,1)S(1)}, ...), condition=%wide.region_6.7_spmd, body=%wide.region_0.6_spmd.sunk | while | flops 591418240 | bytes 15384447 | solution.py:162
  15.9 15.2 %all_gather.24 = bf16[128,2048]{0,1:T(8,128)(2,1)S(1)} all-gather(bf16[128,256]{0,1:T(8,128)(2,1)S(1)} %broadcast_select_fusion.3), channel_id=1, replica_groups=mesh['pp'=4,'tp'=8] {'tp'}, dimensions={1}, use_global_device_ids=true | all-gather | bytes 589824 | tf_op jit(solution)/shard_map/while/body/eval_jaxpr/all_gather | solution.py:123
  31.4 4.2 %convolution_multiply_fusion.2 = f32[128,1024]{1,0:T(8,128)S(1)} fusion(bf16[1024,2048]{1,0:T(8,128)(2,1)} %get-tuple-element.745, bf16[128,2048]{0,1:T(8,128)(2,1)S(1)} %all_gather.24, f32[2048]{0:T(1024)S(1)} %bitcast.155, f32[128]{0:T(128)S(1)} %add_rsqrt_fusion.4), kind=kOutput, calls=%fused_computation.26.clone.1 | convolution fusion | flops 537788416 | bytes 5251584 | tf_op jit(solution)/shard_map/while/body/eval_jaxpr/dot_general | solution.py:112
  37.1 5.0 %while.60 = (s32[]{:T(128)}, f32[4,64,64]{2,1,0:T(8,128)S(1)}, f32[2,4,64,64]{3,2,1,0:T(8,128)S(1)}, f32[2,4,64,64]{2,0,3,1:T(2,128)S(1)}, f32[2,4,64,64]{2,0,3,...) while((s32[]{:T(128)}, f32[4,64,64]{2,1,0:T(8,128)S(1)}, ...), condition=%wide.region_4.4_spmd.clone, body=%wide.region_2.3_spmd.clone.sunk | while | flops 51564544 | bytes 2504832 | solution.py:51
  43.0 3.4 %collective-permute-start = (bf16[128,256]{0,1:T(8,128)(2,1)S(1)}, bf16[128,256]{0,1:T(8,128)(2,1)S(1)}, u32[]{:S(2)}, u32[]{:S(2)}) collective-permute-start(bf16[128,256]{0,1:T(8,128)(2,1)S(1)} %get-tuple-element.651), channel_id=1, source_target_pairs={{0,8},{8,16},{16,24},{1,9},{9,17},{17,25},{2,10},{10,18},{18,26},{... | collective-permute-start | bytes 196616 | tf_op jit(solution)/shard_map/while/body/eval_jaxpr/ppermute | solution.py:15
  48.4 14.7 %all_gather.24 = bf16[128,2048]{0,1:T(8,128)(2,1)S(1)} all-gather(bf16[128,256]{0,1:T(8,128)(2,1)S(1)} %broadcast_select_fusion.3), channel_id=1, replica_groups=mesh['pp'=4,'tp'=8] {'tp'}, dimensions={1}, use_global_device_ids=true | all-gather | bytes 589824 | tf_op jit(solution)/shard_map/while/body/eval_jaxpr/all_gather | solution.py:123
  63.4 4.2 %convolution_multiply_fusion.2 = f32[128,1024]{1,0:T(8,128)S(1)} fusion(bf16[1024,2048]{1,0:T(8,128)(2,1)} %get-tuple-element.745, bf16[128,2048]{0,1:T(8,128)(2,1)S(1)} %all_gather.24, f32[2048]{0:T(1024)S(1)} %bitcast.155, f32[128]{0:T(128)S(1)} %add_rsqrt_fusion.4), kind=kOutput, calls=%fused_computation.26.clone.1 | convolution fusion | flops 537788416 | bytes 5251584 | tf_op jit(solution)/shard_map/while/body/eval_jaxpr/dot_general | solution.py:112
  69.2 5.0 %while.60 = (s32[]{:T(128)}, f32[4,64,64]{2,1,0:T(8,128)S(1)}, f32[2,4,64,64]{3,2,1,0:T(8,128)S(1)}, f32[2,4,64,64]{2,0,3,1:T(2,128)S(1)}, f32[2,4,64,64]{2,0,3,...) while((s32[]{:T(128)}, f32[4,64,64]{2,1,0:T(8,128)S(1)}, ...), condition=%wide.region_4.4_spmd.clone, body=%wide.region_2.3_spmd.clone.sunk | while | flops 51564544 | bytes 2504832 | solution.py:51
  75.1 4.3 %collective-permute-start = (bf16[128,256]{0,1:T(8,128)(2,1)S(1)}, bf16[128,256]{0,1:T(8,128)(2,1)S(1)}, u32[]{:S(2)}, u32[]{:S(2)}) collective-permute-start(bf16[128,256]{0,1:T(8,128)(2,1)S(1)} %get-tuple-element.651), channel_id=1, source_target_pairs={{0,8},{8,16},{16,24},{1,9},{9,17},{17,25},{2,10},{10,18},{18,26},{... | collective-permute-start | bytes 196616 | tf_op jit(solution)/shard_map/while/body/eval_jaxpr/ppermute | solution.py:15
  81.5 15.0 %all_gather.24 = bf16[128,2048]{0,1:T(8,128)(2,1)S(1)} all-gather(bf16[128,256]{0,1:T(8,128)(2,1)S(1)} %broadcast_select_fusion.3), channel_id=1, replica_groups=mesh['pp'=4,'tp'=8] {'tp'}, dimensions={1}, use_global_device_ids=true | all-gather | bytes 589824 | tf_op jit(solution)/shard_map/while/body/eval_jaxpr/all_gather | solution.py:123
  96.8 4.2 %convolution_multiply_fusion.2 = f32[128,1024]{1,0:T(8,128)S(1)} fusion(bf16[1024,2048]{1,0:T(8,128)(2,1)} %get-tuple-element.745, bf16[128,2048]{0,1:T(8,128)(2,1)S(1)} %all_gather.24, f32[2048]{0:T(1024)S(1)} %bitcast.155, f32[128]{0:T(128)S(1)} %add_rsqrt_fusion.4), kind=kOutput, calls=%fused_computation.26.clone.1 | convolution fusion | flops 537788416 | bytes 5251584 | tf_op jit(solution)/shard_map/while/body/eval_jaxpr/dot_general | solution.py:112
  102.5 5.0 %while.60 = (s32[]{:T(128)}, f32[4,64,64]{2,1,0:T(8,128)S(1)}, f32[2,4,64,64]{3,2,1,0:T(8,128)S(1)}, f32[2,4,64,64]{2,0,3,1:T(2,128)S(1)}, f32[2,4,64,64]{2,0,3,...) while((s32[]{:T(128)}, f32[4,64,64]{2,1,0:T(8,128)S(1)}, ...), condition=%wide.region_4.4_spmd.clone, body=%wide.region_2.3_spmd.clone.sunk | while | flops 51564544 | bytes 2504832 | solution.py:51
  108.4 4.3 %collective-permute-start = (bf16[128,256]{0,1:T(8,128)(2,1)S(1)}, bf16[128,256]{0,1:T(8,128)(2,1)S(1)}, u32[]{:S(2)}, u32[]{:S(2)}) collective-permute-start(bf16[128,256]{0,1:T(8,128)(2,1)S(1)} %get-tuple-element.651), channel_id=1, source_target_pairs={{0,8},{8,16},{16,24},{1,9},{9,17},{17,25},{2,10},{10,18},{18,26},{... | collective-permute-start | bytes 196616 | tf_op jit(solution)/shard_map/while/body/eval_jaxpr/ppermute | solution.py:15
  114.7 15.0 %all_gather.24 = bf16[128,2048]{0,1:T(8,128)(2,1)S(1)} all-gather(bf16[128,256]{0,1:T(8,128)(2,1)S(1)} %broadcast_select_fusion.3), channel_id=1, replica_groups=mesh['pp'=4,'tp'=8] {'tp'}, dimensions={1}, use_global_device_ids=true | all-gather | bytes 589824 | tf_op jit(solution)/shard_map/while/body/eval_jaxpr/all_gather | solution.py:123
  130.0 4.2 %convolution_multiply_fusion.2 = f32[128,1024]{1,0:T(8,128)S(1)} fusion(bf16[1024,2048]{1,0:T(8,128)(2,1)} %get-tuple-element.745, bf16[128,2048]{0,1:T(8,128)(2,1)S(1)} %all_gather.24, f32[2048]{0:T(1024)S(1)} %bitcast.155, f32[128]{0:T(128)S(1)} %add_rsqrt_fusion.4), kind=kOutput, calls=%fused_computation.26.clone.1 | convolution fusion | flops 537788416 | bytes 5251584 | tf_op jit(solution)/shard_map/while/body/eval_jaxpr/dot_general | solution.py:112
  135.8 5.0 %while.60 = (s32[]{:T(128)}, f32[4,64,64]{2,1,0:T(8,128)S(1)}, f32[2,4,64,64]{3,2,1,0:T(8,128)S(1)}, f32[2,4,64,64]{2,0,3,1:T(2,128)S(1)}, f32[2,4,64,64]{2,0,3,...) while((s32[]{:T(128)}, f32[4,64,64]{2,1,0:T(8,128)S(1)}, ...), condition=%wide.region_4.4_spmd.clone, body=%wide.region_2.3_spmd.clone.sunk | while | flops 51564544 | bytes 2504832 | solution.py:51
  141.6 5.1 %collective-permute-start = (bf16[128,256]{0,1:T(8,128)(2,1)S(1)}, bf16[128,256]{0,1:T(8,128)(2,1)S(1)}, u32[]{:S(2)}, u32[]{:S(2)}) collective-permute-start(bf16[128,256]{0,1:T(8,128)(2,1)S(1)} %get-tuple-element.651), channel_id=1, source_target_pairs={{0,8},{8,16},{16,24},{1,9},{9,17},{17,25},{2,10},{10,18},{18,26},{... | collective-permute-start | bytes 196616 | tf_op jit(solution)/shard_map/while/body/eval_jaxpr/ppermute | solution.py:15
  148.8 14.9 %all_gather.24 = bf16[128,2048]{0,1:T(8,128)(2,1)S(1)} all-gather(bf16[128,256]{0,1:T(8,128)(2,1)S(1)} %broadcast_select_fusion.3), channel_id=1, replica_groups=mesh['pp'=4,'tp'=8] {'tp'}, dimensions={1}, use_global_device_ids=true | all-gather | bytes 589824 | tf_op jit(solution)/shard_map/while/body/eval_jaxpr/all_gather | solution.py:123
  164.0 4.2 %convolution_multiply_fusion.2 = f32[128,1024]{1,0:T(8,128)S(1)} fusion(bf16[1024,2048]{1,0:T(8,128)(2,1)} %get-tuple-element.745, bf16[128,2048]{0,1:T(8,128)(2,1)S(1)} %all_gather.24, f32[2048]{0:T(1024)S(1)} %bitcast.155, f32[128]{0:T(128)S(1)} %add_rsqrt_fusion.4), kind=kOutput, calls=%fused_computation.26.clone.1 | convolution fusion | flops 537788416 | bytes 5251584 | tf_op jit(solution)/shard_map/while/body/eval_jaxpr/dot_general | solution.py:112
  169.8 5.0 %while.60 = (s32[]{:T(128)}, f32[4,64,64]{2,1,0:T(8,128)S(1)}, f32[2,4,64,64]{3,2,1,0:T(8,128)S(1)}, f32[2,4,64,64]{2,0,3,1:T(2,128)S(1)}, f32[2,4,64,64]{2,0,3,...) while((s32[]{:T(128)}, f32[4,64,64]{2,1,0:T(8,128)S(1)}, ...), condition=%wide.region_4.4_spmd.clone, body=%wide.region_2.3_spmd.clone.sunk | while | flops 51564544 | bytes 2504832 | solution.py:51
  175.7 5.2 %collective-permute-start = (bf16[128,256]{0,1:T(8,128)(2,1)S(1)}, bf16[128,256]{0,1:T(8,128)(2,1)S(1)}, u32[]{:S(2)}, u32[]{:S(2)}) collective-permute-start(bf16[128,256]{0,1:T(8,128)(2,1)S(1)} %get-tuple-element.651), channel_id=1, source_target_pairs={{0,8},{8,16},{16,24},{1,9},{9,17},{17,25},{2,10},{10,18},{18,26},{... | collective-permute-start | bytes 196616 | tf_op jit(solution)/shard_map/while/body/eval_jaxpr/ppermute | solution.py:15
  182.8 16.3 %all-gather = bf16[1024,256]{0,1:T(8,128)(2,1)S(1)} all-gather(bf16[256,256]{0,1:T(8,128)(2,1)S(1)} %broadcast_select_fusion.1), channel_id=2, replica_groups=mesh['pp'=4,'tp'=8] {'pp'}, dimensions={0}, use_global_device_ids=true | all-gather | bytes 655360 | tf_op jit(solution)/shard_map/all_gather | solution.py:20
  (299 shorter events, 50.8 us)
Async XLA Ops:
  2.0 3.8 %copy-start.2 = (bf16[64,256]{1,0:T(8,128)(2,1)S(1)}, bf16[64,256]{1,0:T(8,128)(2,1)}, u32[]{:S(2)}) copy-start(bf16[64,256]{1,0:T(8,128)(2,1)} %param.13) | copy-start | bytes 98308
  2.0 13.7 %copy-start = (f32[1,2048]{1,0:T(1,128)S(1)}, f32[1,2048]{1,0:T(1,128)}, u32[]{:S(2)}) copy-start(f32[1,2048]{1,0:T(1,128)} %param.14) | copy-start | bytes 24580
  2.0 13.7 %copy-start.1 = (f32[1,128,4]{1,2,0:T(4,128)S(1)}, f32[1,128,4]{1,2,0:T(4,128)}, u32[]{:S(2)}) copy-start(f32[1,128,4]{1,2,0:T(4,128)} %param.20) | copy-start | bytes 6148
  2.0 13.7 %copy-start.3 = (f32[1,64]{1,0:T(1,128)S(1)}, f32[1,64]{1,0:T(1,128)}, u32[]{:S(2)}) copy-start(f32[1,64]{1,0:T(1,128)} %param.21) | copy-start | bytes 772
  43.0 5.3 %collective-permute-start = (bf16[128,256]{0,1:T(8,128)(2,1)S(1)}, bf16[128,256]{0,1:T(8,128)(2,1)S(1)}, u32[]{:S(2)}, u32[]{:S(2)}) collective-permute-start(bf16[128,256]{0,1:T(8,128)(2,1)S(1)} %get-tuple-element.651), channel_id=1, source_target_pairs={{0,8},{8,16},{16,24},{1,9},{9,17},{17,25},{2,10},{10,18},{18,26},{... | collective-permute-start | bytes 196616 | tf_op jit(solution)/shard_map/while/body/eval_jaxpr/ppermute | solution.py:15
  75.1 6.2 %collective-permute-start = (bf16[128,256]{0,1:T(8,128)(2,1)S(1)}, bf16[128,256]{0,1:T(8,128)(2,1)S(1)}, u32[]{:S(2)}, u32[]{:S(2)}) collective-permute-start(bf16[128,256]{0,1:T(8,128)(2,1)S(1)} %get-tuple-element.651), channel_id=1, source_target_pairs={{0,8},{8,16},{16,24},{1,9},{9,17},{17,25},{2,10},{10,18},{18,26},{... | collective-permute-start | bytes 196616 | tf_op jit(solution)/shard_map/while/body/eval_jaxpr/ppermute | solution.py:15
  108.4 6.2 %collective-permute-start = (bf16[128,256]{0,1:T(8,128)(2,1)S(1)}, bf16[128,256]{0,1:T(8,128)(2,1)S(1)}, u32[]{:S(2)}, u32[]{:S(2)}) collective-permute-start(bf16[128,256]{0,1:T(8,128)(2,1)S(1)} %get-tuple-element.651), channel_id=1, source_target_pairs={{0,8},{8,16},{16,24},{1,9},{9,17},{17,25},{2,10},{10,18},{18,26},{... | collective-permute-start | bytes 196616 | tf_op jit(solution)/shard_map/while/body/eval_jaxpr/ppermute | solution.py:15
  141.6 7.0 %collective-permute-start = (bf16[128,256]{0,1:T(8,128)(2,1)S(1)}, bf16[128,256]{0,1:T(8,128)(2,1)S(1)}, u32[]{:S(2)}, u32[]{:S(2)}) collective-permute-start(bf16[128,256]{0,1:T(8,128)(2,1)S(1)} %get-tuple-element.651), channel_id=1, source_target_pairs={{0,8},{8,16},{16,24},{1,9},{9,17},{17,25},{2,10},{10,18},{18,26},{... | collective-permute-start | bytes 196616 | tf_op jit(solution)/shard_map/while/body/eval_jaxpr/ppermute | solution.py:15
  175.7 7.1 %collective-permute-start = (bf16[128,256]{0,1:T(8,128)(2,1)S(1)}, bf16[128,256]{0,1:T(8,128)(2,1)S(1)}, u32[]{:S(2)}, u32[]{:S(2)}) collective-permute-start(bf16[128,256]{0,1:T(8,128)(2,1)S(1)} %get-tuple-element.651), channel_id=1, source_target_pairs={{0,8},{8,16},{16,24},{1,9},{9,17},{17,25},{2,10},{10,18},{18,26},{... | collective-permute-start | bytes 196616 | tf_op jit(solution)/shard_map/while/body/eval_jaxpr/ppermute | solution.py:15
